TPU v7x, 32 devices: a whole 2x2x4 slice. The times are simulated.
32 devices in a mesh: grp: 2 (over y), sp: 4 (over z), tp: 4 (over x, core).
Axes of the slice: x: 2, y: 2, z: 4, core: 2. Of those that a mesh axis runs over, the one named last changes fastest.
Arguments:
- tokens: bfloat16 [4096, 2048], P(('grp', 'sp'), 'tp'), parts along dimension 0, may hold values from -140 to 140, as said below
- mix_gain: bfloat16 [2, 2048], replicated, may hold values from 0.099609375 to 1.8984375
- gate_weight: bfloat16 [2, 2048, 2048], P(None, 'sp', 'tp'), may hold values from -0.125 to 0.125
- mix_weight: bfloat16 [2, 2048, 2048], P(None, 'sp', 'tp'), may hold values from -0.125 to 0.125
- value_weight: bfloat16 [2, 2048, 2048], P(None, 'sp', 'tp'), may hold values from -0.125 to 0.125
- out_weight: bfloat16 [2, 2048, 2048], P(None, 'sp', 'tp'), may hold values from -0.125 to 0.125
- conv_taps: bfloat16 [2, 3, 2048], P(None, None, 'tp'), may hold values from -3.5 to 3.5
Outputs:
- result_stream: bfloat16 [4096, 2048], P(('grp', 'sp'), 'tp'), parts along dimension 0
There are 2 independent parts, one for each index of `grp`. A program takes and returns all parts, laid end to end along the dimension named above; an argument that names none is the same for every part. Nothing has to cross between parts.
Inputs may be any that keep to these rules, and one draw needn't show every extreme that they name: `tokens`: activations with feature scales of several sizes.
All inputs are finite; a program needn't handle non-finite values.
Results may differ from a plain program's by a relative error of at most 0.015.
Values may be sent and summed in bfloat16 or wider, within the bound.
A program may use at most 64 MiB of HBM per device.

v0:
```python
import jax
import jax.numpy as jnp
from jax import lax
from jax.sharding import PartitionSpec as P

EPS = 1e-06


def passed_along(x, axis, by):
    devices = lax.axis_size(axis)
    pairs = [(i, i + by) for i in range(devices) if 0 <= i + by < devices]
    return lax.ppermute(x, axis, pairs)


def normed_rows(rows, gain):
    wide_rows = rows.astype(jnp.float32)
    factor = lax.rsqrt(jnp.mean(wide_rows * wide_rows, axis=1, keepdims=True) + EPS)
    return (wide_rows * factor * gain.astype(jnp.float32)).astype(jnp.bfloat16)


def convolve(carried, before, tap_rows):
    padded = jnp.concatenate([before, carried], axis=0)
    row_count = carried.shape[0]
    result = jnp.zeros_like(carried)
    for tap_index in range(tap_rows.shape[0]):
        result = (
            result
            + tap_rows[tap_index].astype(jnp.float32) * padded[tap_index : tap_index + row_count]
        )
    return result


def shards(tokens, mix_gain, gate_weight, mix_weight, value_weight, out_weight, conv_taps):
    layer_count = gate_weight.shape[0]
    conv_reach = conv_taps.shape[1] - 1
    fringe_depth = 0
    stream = tokens
    gathered = (
        lax.all_gather(gate_weight, "sp", axis=1, tiled=True),
        lax.all_gather(mix_weight, "sp", axis=1, tiled=True),
        lax.all_gather(value_weight, "sp", axis=1, tiled=True),
        lax.all_gather(out_weight, "sp", axis=1, tiled=True),
    )
    for layer_index in range(layer_count):
        whole = lax.all_gather(stream, "tp", axis=1, tiled=True)
        normed = normed_rows(whole, mix_gain[layer_index])
        gate = jnp.dot(normed, gathered[0][layer_index], preferred_element_type=jnp.float32)
        inner = jnp.dot(normed, gathered[1][layer_index], preferred_element_type=jnp.float32)
        values = jnp.dot(normed, gathered[2][layer_index], preferred_element_type=jnp.float32)
        gate = gate.astype(jnp.bfloat16)
        inner = inner.astype(jnp.bfloat16)
        values = values.astype(jnp.bfloat16)
        carried = inner.astype(jnp.float32) * values.astype(jnp.float32)
        before = passed_along(carried[carried.shape[0] - conv_reach :], "sp", 1)
        conv = convolve(carried, before, conv_taps[layer_index])
        mixed = (gate.astype(jnp.float32) * conv).astype(jnp.bfloat16)
        mixed_all = lax.all_gather(mixed, "tp", axis=1, tiled=True)
        product = jnp.dot(mixed_all, gathered[3][layer_index], preferred_element_type=jnp.float32)
        stream = (stream.astype(jnp.float32) + product).astype(jnp.bfloat16)
    return stream


def solution(mesh):
    return jax.shard_map(
        shards,
        mesh=mesh,
        in_specs=(
            P(("grp", "sp"), "tp"),
            P(),
            P(None, "sp", "tp"),
            P(None, "sp", "tp"),
            P(None, "sp", "tp"),
            P(None, "sp", "tp"),
            P(None, None, "tp"),
        ),
        out_specs=P(("grp", "sp"), "tp"),
        check_vma=False,
    )
```

profile of v0, /device:TPU:0, one launch (start us, length us, event | category | flops | bytes accessed | tf_op | source)
XLA Modules:
  0.0 456.6 jit_solution(16903297331807922796)
XLA Ops:
  6.5 0.7 all-gather.9.cloned.1.call-update
  7.3 0.0 all-gather.15.cloned.1.call-start
  7.3 0.7 all-gather.15.cloned.1.call-update
  8.0 0.0 all-gather.13.cloned.1.call-start
  8.1 0.7 all-gather.13.cloned.1.call-update
  8.8 0.0 all-gather.11.cloned.1.call-start
  8.8 0.5 all-gather.11.cloned.1.call-update
  9.4 0.5 all-gather.19.cloned.1.call-update
  9.9 0.0 all-gather.17.cloned.1.call-start
  10.0 24.2 %all-gather.9.cloned.1.call-done = bf16[512,2048]{1,0:T(8,128)(2,1)} async-done(((bf16[512,512]{1,0:T(8,128)(2,1)}), bf16[512,2048]{1,0:T(8,128)(2,1)}) %all-gather.9.cloned.1.call-update) | async-done | bytes 2097168 | tf_op jit(solution)/shard_map/all_gather | solution.py:45
  34.2 2.2 fusion
  36.4 80.1 %all-gather.15.cloned.1.call-done = bf16[2,2048,512]{2,1,0:T(8,128)(2,1)} async-done(((bf16[2,512,512]{2,1,0:T(8,128)(2,1)}), bf16[2,2048,512]{2,1,0:T(8,128)(2,1)}) %all-gather.15.cloned.1.call-update) | async-done | bytes 4194320 | tf_op jit(solution)/shard_map/all_gather | solution.py:41
  116.6 2.9 fusion.22
  119.5 77.9 %all-gather.13.cloned.1.call-done = bf16[2,2048,512]{2,1,0:T(8,128)(2,1)} async-done(((bf16[2,512,512]{2,1,0:T(8,128)(2,1)}), bf16[2,2048,512]{2,1,0:T(8,128)(2,1)}) %all-gather.13.cloned.1.call-update) | async-done | bytes 4194320 | tf_op jit(solution)/shard_map/all_gather | solution.py:40
  197.4 2.9 fusion.20
  200.3 1.3 collective-permute-start
  201.7 76.4 %all-gather.11.cloned.1.call-done = bf16[2,2048,512]{2,1,0:T(8,128)(2,1)} async-done(((bf16[2,512,512]{2,1,0:T(8,128)(2,1)}), bf16[2,2048,512]{2,1,0:T(8,128)(2,1)}) %all-gather.11.cloned.1.call-update) | async-done | bytes 4194320 | tf_op jit(solution)/shard_map/all_gather | solution.py:39
  278.1 4.9 %fusion.43 = bf16[512,512]{1,0:T(8,128)(2,1)} fusion(f32[2,512]{1,0:T(2,128)S(1)} %collective-permute-done, f32[512,512]{1,0:T(8,128)} %copy-done.6, f32[512]{0:T(512)S(1)} %bitcast.83, f32[512]{0:T(512)S(1)} %bitcast.84, f32[512]{0:T(512)S(1)} %bitcast.85, bf16[2,2048,512]{2,1,0:T(8,128)(2,1)} %all-gather.11.cloned.1.call-done, ...), kind=kOutput, calls=%fused_computation.59 | convolution fusion | flops 1080819712 | bytes 5787648 | tf_op jit(solution)/shard_map/dot_general | solution.py:47
  283.0 0.0 all-gather.21.cloned.1.call-start
  283.1 75.7 %all-gather.19.cloned.1.call-done = bf16[2,2048,512]{2,1,0:T(8,128)(2,1)} async-done(((bf16[2,512,512]{2,1,0:T(8,128)(2,1)}), bf16[2,2048,512]{2,1,0:T(8,128)(2,1)}) %all-gather.19.cloned.1.call-update) | async-done | bytes 4194320 | tf_op jit(solution)/shard_map/all_gather | solution.py:42
  358.7 22.5 %all-gather.17.cloned.1.call-done = bf16[512,2048]{1,0:T(8,128)(2,1)} async-done(((bf16[512,512]{1,0:T(8,128)(2,1)}), bf16[512,2048]{1,0:T(8,128)(2,1)}) %all-gather.17.cloned.1.call-update) | async-done | bytes 2097168 | tf_op jit(solution)/shard_map/all_gather | solution.py:57
  381.2 4.3 fusion.31
  385.5 0.0 all-gather.23.cloned.1.call-start
  385.6 22.7 %all-gather.21.cloned.1.call-done = bf16[512,2048]{1,0:T(8,128)(2,1)} async-done(((bf16[512,512]{1,0:T(8,128)(2,1)}), bf16[512,2048]{1,0:T(8,128)(2,1)}) %all-gather.21.cloned.1.call-update) | async-done | bytes 2097168 | tf_op jit(solution)/shard_map/all_gather | solution.py:45
  408.3 2.2 fusion.3
  410.5 3.0 fusion.29
  413.6 1.3 fusion.27
  414.9 3.4 collective-permute-start.1
  418.3 1.3 collective-permute-done.1
  419.7 2.3 fusion.37
  422.0 23.5 %all-gather.23.cloned.1.call-done = bf16[512,2048]{1,0:T(8,128)(2,1)} async-done(((bf16[512,512]{1,0:T(8,128)(2,1)}), bf16[512,2048]{1,0:T(8,128)(2,1)}) %all-gather.23.cloned.1.call-update) | async-done | bytes 2097168 | tf_op jit(solution)/shard_map/all_gather | solution.py:57
  445.5 4.3 fusion.30
  (30 shorter events, 0.2 us)
Async XLA Ops:
  6.5 27.7 %all-gather.9.cloned.1.call-start = ((), (), s32[]{:S(2)}) async-start(), calls=%async_computation | async-start | bytes 2621440 | tf_op jit(solution)/shard_map/all_gather | solution.py:45
  7.3 2.7 copy-start.4
  7.3 109.3 %all-gather.15.cloned.1.call-start = ((), (), s32[]{:S(2)}) async-start(), calls=%async_computation.3 | async-start | bytes 5242880 | tf_op jit(solution)/shard_map/all_gather | solution.py:41
  8.0 189.4 %all-gather.13.cloned.1.call-start = ((), (), s32[]{:S(2)}) async-start(), calls=%async_computation.2 | async-start | bytes 5242880 | tf_op jit(solution)/shard_map/all_gather | solution.py:40
  8.8 269.3 %all-gather.11.cloned.1.call-start = ((), (), s32[]{:S(2)}) async-start(), calls=%async_computation.1 | async-start | bytes 5242880 | tf_op jit(solution)/shard_map/all_gather | solution.py:39
  9.3 349.4 %all-gather.19.cloned.1.call-start = ((), (), s32[]{:S(2)}) async-start(), calls=%async_computation.5 | async-start | bytes 5242880 | tf_op jit(solution)/shard_map/all_gather | solution.py:42
  9.9 371.3 %all-gather.17.cloned.1.call-start = ((), (), s32[]{:S(2)}) async-start(), calls=%async_computation.4 | async-start | bytes 2621440 | tf_op jit(solution)/shard_map/all_gather | solution.py:57
  34.2 82.3 %copy-start = (bf16[512,2048]{1,0:T(8,128)(2,1)S(1)}, bf16[512,2048]{1,0:T(8,128)(2,1)}, u32[]{:S(2)}) copy-start(bf16[512,2048]{1,0:T(8,128)(2,1)} %all-gather.9.cloned.1.call-done) | copy-start | bytes 6291460
  119.5 82.2 %copy-start.5 = (bf16[2,3,512]{2,0,1:T(2,128)(2,1)S(1)}, bf16[2,3,512]{2,0,1:T(2,128)(2,1)}, u32[]{:S(2)}) copy-start(bf16[2,3,512]{2,0,1:T(2,128)(2,1)} %param.13) | copy-start | bytes 18436
  200.3 1.3 copy-start.6
  200.3 77.8 %collective-permute-start = (f32[2,512]{1,0:T(2,128)S(1)}, f32[2,512]{1,0:T(2,128)S(1)}, u32[]{:S(2)}, u32[]{:S(2)}) collective-permute-start(f32[2,512]{1,0:T(2,128)S(1)} %slice.105), channel_id=1, source_target_pairs={{0,4},{4,8},{8,12},{1,5},{5,9},{9,13},{2,6},{6,10},{10,14},{3,7},{... | collective-permute-start | bytes 12296 | tf_op jit(solution)/shard_map/ppermute | solution.py:12
  278.1 103.2 %copy-start.2 = (bf16[512,512]{1,0:T(8,128)(2,1)S(1)}, bf16[512,512]{1,0:T(8,128)(2,1)}, u32[]{:S(2)}) copy-start(bf16[512,512]{1,0:T(8,128)(2,1)} %param.7) | copy-start | bytes 1572868
  283.0 125.2 %all-gather.21.cloned.1.call-start = ((), (), s32[]{:S(2)}) async-start(), calls=%async_computation.6 | async-start | bytes 2621440 | tf_op jit(solution)/shard_map/all_gather | solution.py:45
  385.5 60.0 %all-gather.23.cloned.1.call-start = ((), (), s32[]{:S(2)}) async-start(), calls=%async_computation.7 | async-start | bytes 2621440 | tf_op jit(solution)/shard_map/all_gather | solution.py:57
  408.3 2.2 copy-start.1
  410.5 3.1 copy-start.8
  413.6 6.1 %copy-start.7 = (bf16[2,2048,512]{2,1,0:T(8,128)(2,1)S(1)}, bf16[2,2048,512]{2,1,0:T(8,128)(2,1)}, u32[]{:S(2)}) copy-start(bf16[2,2048,512]{2,1,0:T(8,128)(2,1)} %all-gather.11.cloned.1.call-done) | copy-start | bytes 12582916
  414.9 4.7 %collective-permute-start.1 = (f32[2,512]{1,0:T(2,128)S(1)}, f32[2,512]{1,0:T(2,128)S(1)}, u32[]{:S(2)}, u32[]{:S(2)}) collective-permute-start(f32[2,512]{1,0:T(2,128)S(1)} %slice.112), channel_id=1, source_target_pairs={{0,4},{4,8},{8,12},{1,5},{5,9},{9,13},{2,6},{6,10},{10,14},{3,7},{... | collective-permute-start | bytes 12296 | tf_op jit(solution)/shard_map/ppermute | solution.py:12
  419.6 25.9 %copy-start.3 = (bf16[512,512]{1,0:T(8,128)(2,1)S(1)}, bf16[512,512]{1,0:T(8,128)(2,1)}, u32[]{:S(2)}) copy-start(bf16[512,512]{1,0:T(8,128)(2,1)} %fusion.31) | copy-start | bytes 1572868
Sparse Core Ops, SparseCore 0:
  8.9 25.2 all-gather.8
  35.8 80.7 all-gather.14
  118.1 79.2 all-gather.12
  198.8 79.2 all-gather.10
  279.5 79.2 all-gather.18
  360.2 21.0 all-gather.16
  385.7 22.5 all-gather.20
  422.1 23.3 all-gather.22
where the time goes:
time: 457 us
  waiting for transfers between devices  408 us (89%)
  matrix products  25.9 us (6%)
  between operations  13.6 us (3%)
  starting transfers between devices  4.96 us (1%)
    all_gather x1, waiting for transfers between devices, shards(): lax.all_gather(value_weight, 'sp', axis=1, tiled=True)  80.1 us
    all_gather x1, waiting for transfers between devices, shards(): lax.all_gather(mix_weight, 'sp', axis=1, tiled=True)  77.9 us
    all_gather x1, waiting for transfers between devices, shards(): lax.all_gather(gate_weight, 'sp', axis=1, tiled=True)  76.4 us
    all_gather x1, waiting for transfers between devices, shards(): lax.all_gather(out_weight, 'sp', axis=1, tiled=True)  75.7 us
    all_gather x2, waiting for transfers between devices, shards(): whole = lax.all_gather(stream, 'tp', axis=1, tiled=True)  46.9 us
    all_gather x2, waiting for transfers between devices, shards(): mixed_all = lax.all_gather(mixed, 'tp', axis=1, tiled=True)  46 us
  transfers between devices with their start and end apart: 10, of which 9 were waited for; matrix products, arithmetic and copies ran while one was open for 3% of the time, Pallas kernels for 0%

commit v1 on v0

v1 whole, which is shorter than its diff:
```python
import functools

import jax
import jax.numpy as jnp
from jax import lax
from jax.experimental import pallas as pl
from jax.experimental.pallas import tpu as pltpu
from jax.sharding import PartitionSpec as P

EPS = 1e-06
KINDS = 4
MESH = pl.DeviceIdType.MESH


def kernel(sizes, tokens, gain, gate_w, mix_w, value_w, out_w, taps, result,
           wide, acts, carried, gates, edge_out, edge_in, last, swap_in,
           local_sem, w_send, w_recv, a_send, a_recv, e_send, e_recv, r_send, r_recv):
    groups, n, tps, lows = sizes
    highs = tps // lows
    rows, block_width = tokens.shape
    layers = gate_w.shape[0]
    depth = gate_w.shape[1]
    width = block_width // groups
    all_rows = groups * rows
    reach = edge_in.shape[2]
    chunk = min(rows, 256)
    me, my_grp, my_tp = lax.axis_index("sp"), lax.axis_index("grp"), lax.axis_index("tp")
    my_high, my_low = my_tp // lows, lax.rem(my_tp, lows)

    def tp_at(high, low):
        return lax.rem(high + highs, highs) * lows + low

    x_next, x_prev = {"tp": tp_at(my_high + 1, my_low)}, {"tp": tp_at(my_high - 1 + highs, my_low)}
    across = {"grp": lax.rem(my_grp + 1, groups)}
    sibling = {"tp": my_high * lows + (1 - my_low)}
    right, left = {"sp": me + 1}, {"sp": me - 1}

    barrier = pltpu.get_barrier_semaphore()
    fixed = []
    if highs > 1:
        fixed.append(x_next)
    if highs > 2:
        fixed.append(x_prev)
    if groups > 1:
        fixed.append(across)
    if lows > 1:
        fixed.append(sibling)
    for device in fixed:
        pl.semaphore_signal(barrier, inc=1, device_id=device, device_id_type=MESH)

    @pl.when(me > 0)
    def _():
        pl.semaphore_signal(barrier, inc=1, device_id=left, device_id_type=MESH)

    @pl.when(me < n - 1)
    def _():
        pl.semaphore_signal(barrier, inc=1, device_id=right, device_id_type=MESH)

    weights = (gate_w, mix_w, value_w, out_w)
    own_columns = pl.ds(pl.multiple_of(my_grp * width, width), width)

    def w_rows(origin):
        return pl.ds(pl.multiple_of(origin * depth, depth), depth)

    def token_place(g, t, offset, size):
        return (pl.ds(pl.multiple_of(g * rows + offset, size), size),
                pl.ds(pl.multiple_of(t * block_width, block_width), block_width))

    def column_place(g, t, offset, size):
        return (pl.ds(offset, size), pl.ds(pl.multiple_of(t * block_width + g * width, width), width))

    own = column_place(my_grp, my_tp, 0, all_rows)[1]
    locals_ = [pltpu.make_async_copy(tokens, acts.at[(0,) + token_place(my_grp, my_tp, 0, rows)], local_sem.at[0])]
    for m in range(layers * KINDS):
        locals_.append(pltpu.make_async_copy(
            weights[m % KINDS].at[m // KINDS, :, own_columns], wide.at[m, w_rows(me), :], local_sem.at[m + 1]))
    for copy in locals_:
        copy.start()
    for copy in locals_:
        copy.wait()

    pl.semaphore_wait(barrier, len(fixed) + jnp.minimum(me, 1) + jnp.minimum(n - 1 - me, 1))

    def w_copy(m, origin, way):
        ref = wide.at[m, w_rows(origin), :]
        return pltpu.make_async_remote_copy(
            src_ref=ref, dst_ref=ref, send_sem=w_send.at[m, way, origin], recv_sem=w_recv.at[m, origin],
            device_id=right if way == 0 else left, device_id_type=MESH)

    def w_own(m):
        @pl.when(me < n - 1)
        def _():
            w_copy(m, me, 0).start()

        @pl.when(me > 0)
        def _():
            w_copy(m, me, 1).start()

    def w_event(m, k):
        @pl.when(me - k >= 0)
        def _():
            w_copy(m, me - k, 0).wait_recv()

            @pl.when(me < n - 1)
            def _():
                w_copy(m, me - k, 0).start()

        @pl.when(me + k < n)
        def _():
            w_copy(m, me + k, 1).wait_recv()

            @pl.when(me > 0)
            def _():
                w_copy(m, me + k, 1).start()

    queue = []
    total = layers * KINDS
    ahead = min(3, total)
    lead = 2 * (n - 1)
    for first in range(0, total, KINDS):
        for part in ((0, 1, 2), (3,)):
            for k in range(1, n):
                for j in part:
                    queue.append((first + j, k))
    state = {"issued": ahead, "done": 0}

    def serve(count):
        while count > 0 and state["done"] < len(queue):
            m, k = queue[state["done"]]
            w_event(m, k)
            state["done"] += 1
            count -= 1
            while state["issued"] < total and queue.index((state["issued"], 1)) <= state["done"] + lead:
                w_own(state["issued"])
                state["issued"] += 1

    def serve_until(m):
        while any(q[0] == m for q in queue[state["done"]:]):
            serve(1)

    sends = []

    def gather(index, place, full, per):
        half = full // 2
        lane = {"next": 0}

        def copy(origin_grp, origin_tp, offset, size, device, slot):
            ref = acts.at[(index,) + place(origin_grp, origin_tp, offset, size)]
            return pltpu.make_async_remote_copy(
                src_ref=ref, dst_ref=ref, send_sem=a_send.at[index, slot], recv_sem=a_recv.at[index, slot],
                device_id=device, device_id_type=MESH)

        def send(g, s, offset, size, device, slot):
            c = copy(lax.rem(my_grp + g, groups), tp_at(my_high - s + highs, my_low), offset, size, device, slot)
            c.start()
            sends.append(c)

        def arrived(g, s, offset, size, slot, low=None):
            low = my_low if low is None else low
            copy(lax.rem(my_grp + g, groups), tp_at(my_high - s + highs, low), offset, size, x_next, slot).wait_recv()

        def to_sibling(g, s, offset, size):
            if lows > 1:
                slot = lane["next"]
                lane["next"] += 1
                send(g, s, offset, size, sibling, slot)
                expected.append((g, s, offset, size, slot))

        expected = []
        base = 5 * highs
        x_slot, y_slot = base, base + highs
        top_slot, low_slot = y_slot + 1, y_slot + 1 + highs
        if highs > 1:
            send(0, 0, 0, full, x_next, x_slot)
        if groups > 1:
            send(0, 0, 0, full, across, y_slot)
        to_sibling(0, 0, 0, full)
        serve(per[0])
        for s in range(1, highs):
            arrived(0, s, 0, full, x_slot + s - 1)
            if groups > 1:
                send(0, s, 0, half, across, top_slot + s - 1)
            if s < highs - 1:
                send(0, s, 0, full, x_next, x_slot + s)
            to_sibling(0, s, 0, full)
        if groups > 1:
            arrived(1, 0, 0, full, y_slot)
            if highs > 1:
                send(1, 0, half, half, x_next, low_slot)
            to_sibling(1, 0, 0, full)
            serve(per[1])
            for s in range(1, highs):
                arrived(1, s, half, half, low_slot + s - 1)
                if s < highs - 1:
                    send(1, s, half, half, x_next, low_slot + s)
                to_sibling(1, s, half, half)
                arrived(1, s, 0, half, top_slot + s - 1)
                to_sibling(1, s, 0, half)
        for g, s, offset, size, slot in expected:
            arrived(g, s, offset, size, slot, 1 - my_low)

    for m in range(ahead):
        w_own(m)
    gather(0, token_place, rows, (2, 1))

    for layer in range(layers):
        now, mixed_at = 2 * layer, 2 * layer + 1
        first = layer * KINDS
        for j in range(3):
            serve_until(first + j)

        def project(g, c):
            start = g * rows + c * chunk
            picked = pl.ds(pl.multiple_of(start, chunk), chunk)
            x = acts[now, picked, :].astype(jnp.float32)
            factor = lax.rsqrt(jnp.mean(x * x, axis=1, keepdims=True) + EPS)
            normed = (x * factor * gain[layer : layer + 1, :].astype(jnp.float32)).astype(jnp.bfloat16)
            gates[picked, :] = jnp.dot(normed, wide[first], preferred_element_type=jnp.float32).astype(jnp.bfloat16)
            inner = jnp.dot(normed, wide[first + 1], preferred_element_type=jnp.float32).astype(jnp.bfloat16)
            values = jnp.dot(normed, wide[first + 2], preferred_element_type=jnp.float32).astype(jnp.bfloat16)
            carried[g, pl.ds(pl.multiple_of(8 + c * chunk, 8), chunk), :] = (
                inner.astype(jnp.float32) * values.astype(jnp.float32))

        chunks = rows // chunk

        @pl.loop(0, groups * chunks)
        def _(i):
            project(lax.rem(i, groups), chunks - 1 - i // groups)

        for g in range(groups):
            edge_out[layer, g] = carried[g, 8 + rows - reach : 8 + rows, :]
        edge = pltpu.make_async_remote_copy(
            src_ref=edge_out.at[layer], dst_ref=edge_in.at[layer], send_sem=e_send.at[layer],
            recv_sem=e_recv.at[layer], device_id=right, device_id_type=MESH)

        @pl.when(me < n - 1)
        def _():
            edge.start()

        @pl.when(me == 0)
        def _():
            for g in range(groups):
                carried[g, 8 - reach : 8, :] = jnp.zeros((reach, width), jnp.float32)

        @pl.when(me > 0)
        def _():
            edge.wait_recv()
            for g in range(groups):
                carried[g, 8 - reach : 8, :] = edge_in[layer, g]

        for g in range(groups):
            conv = jnp.zeros((rows, width), jnp.float32)
            for tap in range(reach + 1):
                row = taps[layer, tap : tap + 1, own_columns].astype(jnp.float32)
                conv = conv + row * carried[g, 8 - reach + tap : 8 - reach + tap + rows, :]
            acts[mixed_at, g * rows : (g + 1) * rows, own] = (
                gates[g * rows : (g + 1) * rows, :].astype(jnp.float32) * conv).astype(jnp.bfloat16)

        gather(mixed_at, column_place, all_rows, (2, 1))
        serve_until(first + 3)

        if layer == 0:
            own_now = pl.ds(pl.multiple_of(my_tp * block_width + my_grp * width, width), width)
        else:
            own_now = own

        @pl.loop(0, all_rows // chunk)
        def _(c):
            picked = pl.ds(pl.multiple_of(c * chunk, chunk), chunk)
            product = jnp.dot(acts[mixed_at, picked, :], wide[first + 3], preferred_element_type=jnp.float32)
            stream = (acts[now, picked, own_now].astype(jnp.float32) + product).astype(jnp.bfloat16)
            if layer < layers - 1:
                acts[now + 2, picked, own] = stream
            else:
                last[picked, :] = stream

        if layer < layers - 1:
            gather(now + 2, column_place, all_rows, (3, 3))

    mine = pl.ds(pl.multiple_of(my_grp * rows, rows), rows)
    if groups > 1:
        other = lax.rem(my_grp + 1, groups)
        final = pltpu.make_async_remote_copy(
            src_ref=last.at[pl.ds(pl.multiple_of(other * rows, rows), rows), :], dst_ref=swap_in,
            send_sem=r_send, recv_sem=r_recv, device_id=across, device_id_type=MESH)
        final.start()
        result[:, own_columns] = last[mine, :]
        final.wait()
        result[:, pl.ds(pl.multiple_of(other * width, width), width)] = swap_in[...]
    else:
        result[...] = last[...]

    serve(len(queue))
    for c in sends:
        c.wait_send()
    for layer in range(layers):
        @pl.when(me < n - 1)
        def _(layer=layer):
            pltpu.make_async_remote_copy(
                src_ref=edge_out.at[layer], dst_ref=edge_in.at[layer], send_sem=e_send.at[layer],
                recv_sem=e_recv.at[layer], device_id=right, device_id_type=MESH).wait_send()
    for m in range(total):
        for k in range(n):
            @pl.when((me - k >= 0) & (me < n - 1))
            def _(m=m, k=k):
                w_copy(m, me - k, 0).wait_send()

            @pl.when((me + k < n) & (me > 0))
            def _(m=m, k=k):
                w_copy(m, me + k, 1).wait_send()


def shards(tokens, mix_gain, gate_weight, mix_weight, value_weight, out_weight, conv_taps):
    groups, n, tps = lax.axis_size("grp"), lax.axis_size("sp"), lax.axis_size("tp")
    assert groups <= 2
    lows = 2 if tps % 2 == 0 else 1
    highs = tps // lows
    rows, block_width = tokens.shape
    layers, depth, _ = gate_weight.shape
    reach = conv_taps.shape[1] - 1
    width = block_width // groups
    all_rows, features = groups * rows, tps * block_width
    slots = 5 * highs + 3 * highs + 1
    total = layers * KINDS
    anywhere = pl.BlockSpec(memory_space=pl.ANY)
    vmem = pl.BlockSpec(memory_space=pltpu.VMEM)
    dma = pltpu.SemaphoreType.DMA
    return pl.pallas_call(
        functools.partial(kernel, (groups, n, tps, lows)),
        out_shape=jax.ShapeDtypeStruct(tokens.shape, tokens.dtype),
        in_specs=[anywhere, vmem, anywhere, anywhere, anywhere, anywhere, vmem],
        out_specs=vmem,
        scratch_shapes=[
            pltpu.VMEM((total, n * depth, width), jnp.bfloat16),
            pltpu.VMEM((2 * layers, all_rows, features), jnp.bfloat16),
            pltpu.VMEM((groups, rows + 8, width), jnp.float32),
            pltpu.VMEM((all_rows, width), jnp.bfloat16),
            pltpu.VMEM((layers, groups, reach, width), jnp.float32),
            pltpu.VMEM((layers, groups, reach, width), jnp.float32),
            pltpu.VMEM((all_rows, width), jnp.bfloat16),
            pltpu.VMEM((rows, width), jnp.bfloat16),
            dma((total + 1,)),
            dma((total, 2, n)),
            dma((total, n)),
            dma((2 * layers, slots)),
            dma((2 * layers, slots)),
            dma((layers,)),
            dma((layers,)),
            dma,
            dma,
        ],
        compiler_params=pltpu.CompilerParams(
            collective_id=0, has_side_effects=True, vmem_limit_bytes=56 * 1024 * 1024
        ),
        name="mixers",
    )(tokens, mix_gain, gate_weight, mix_weight, value_weight, out_weight, conv_taps)


def solution(mesh):
    return jax.shard_map(
        shards,
        mesh=mesh,
        in_specs=(
            P(("grp", "sp"), "tp"),
            P(),
            P(None, "sp", "tp"),
            P(None, "sp", "tp"),
            P(None, "sp", "tp"),
            P(None, "sp", "tp"),
            P(None, None, "tp"),
        ),
        out_specs=P(("grp", "sp"), "tp"),
        check_vma=False,
    )
```

time: 457 us -> 176 us (0.39)
  waiting for transfers between devices: 408 us -> 0 us
  Pallas kernels: 0 us -> 173 us
  matrix products: 25.9 us -> 0 us
  between operations: 13.6 us -> 0.01 us
  starting transfers between devices: 4.96 us -> 0 us
    all_gather x8 -> x0, waiting for transfers between devices: 403 us -> none  [the longest x1 80.1 us: shards(): lax.all_gather(value_weight, 'sp', axis=1, tiled=True)]
    pallas_call x0 -> x1, Pallas kernels: none -> 173 us  [shards(): pl.pallas_call(functools.partial(kernel, (groups, n, tps, lows)), out_sha...]
    dot_general x8 -> x0, matrix products: 25.9 us -> none  [the longest x2 8.54 us: shards(): jnp.dot(mixed_all, gathered[3][layer_index], preferred_element_type=jnp.f...]
    ppermute x2 -> x0, starting transfers between devices: 4.69 us -> none  [passed_along(): return lax.ppermute(x, axis, pairs)]
  transfers between devices with their start and end apart: 10 -> 0, of which waited for: 9 -> 0; matrix products, arithmetic and copies ran while one was open for 3% -> 0% of each run, Pallas kernels for 0% -> 0%
where the time goes in v1:
time: 176 us
  Pallas kernels  173 us (98%)
  local copies, waits for them, and re-layouts  3.16 us (2%)
    pallas_call x1, Pallas kernels, shards(): pl.pallas_call(functools.partial(kernel, (groups, n, tps, lows)), out_sha...  173 us

profile of v1, /device:TPU:0, one launch (start us, length us, event | category | flops | bytes accessed | tf_op | source)
XLA Modules:
  0.0 175.9 jit_solution(16503567077531146315)
XLA Ops:
  0.0 1.3 copy.8.taps
  1.3 172.7 %mixers.1 = bf16[512,512]{1,0:T(8,128)(2,1)} custom-call(bf16[512,512]{1,0:T(8,128)(2,1)} %tokens.1, bf16[2,2048]{1,0:T(2,128)(2,1)} %gain.1, bf16[2,512,512]{2,1,0:T(8,128)(2,1)} %gate_w.1, bf16[2,512,512]{2,1,0:T(8,128)(2,1)} %mix_w.1, bf16[2,512,512]{2,1,0:T(8,128)(2,1)} %value_w.1, bf16[2,512,512]{2,1,0:T(8,128)(2,1)} %out_w.1, bf16[2,3,512]{2,1,0:T(4,128)(2,1)} %copy.8.taps), custom_call_target="tpu_custom_call" | custom-call | tf_op jit(solution)/shard_map/mixers/pallas_call | solution.py:328
  174.0 1.9 %copy.10 = bf16[512,512]{1,0:T(8,128)(2,1)} copy(bf16[512,512]{1,0:T(8,128)(2,1)} %mixers.1) | data formatting | bytes 1048576

commit v2 on v1

--- a/solution.py
+++ b/solution.py
@@ -116,7 +116,7 @@
     queue = []
     total = layers * KINDS
     ahead = min(3, total)
-    lead = 2 * (n - 1)
+    lead = 1 * (n - 1)
     for first in range(0, total, KINDS):
         for part in ((0, 1, 2), (3,)):
             for k in range(1, n):
@@ -140,14 +140,14 @@
 
     sends = []
 
-    def gather(index, place, full, per):
+    def gather(index, sems, place, full):
         half = full // 2
         lane = {"next": 0}
 
         def copy(origin_grp, origin_tp, offset, size, device, slot):
             ref = acts.at[(index,) + place(origin_grp, origin_tp, offset, size)]
             return pltpu.make_async_remote_copy(
-                src_ref=ref, dst_ref=ref, send_sem=a_send.at[index, slot], recv_sem=a_recv.at[index, slot],
+                src_ref=ref, dst_ref=ref, send_sem=a_send.at[sems, slot], recv_sem=a_recv.at[sems, slot],
                 device_id=device, device_id_type=MESH)
 
         def send(g, s, offset, size, device, slot):
@@ -158,6 +158,8 @@
         def arrived(g, s, offset, size, slot, low=None):
             low = my_low if low is None else low
             copy(lax.rem(my_grp + g, groups), tp_at(my_high - s + highs, low), offset, size, x_next, slot).wait_recv()
+
+        expected = []
 
         def to_sibling(g, s, offset, size):
             if lows > 1:
@@ -166,43 +168,63 @@
                 send(g, s, offset, size, sibling, slot)
                 expected.append((g, s, offset, size, slot))
 
-        expected = []
-        base = 5 * highs
-        x_slot, y_slot = base, base + highs
+        x_slot = 5 * highs
+        y_slot = x_slot + highs
         top_slot, low_slot = y_slot + 1, y_slot + 1 + highs
-        if highs > 1:
-            send(0, 0, 0, full, x_next, x_slot)
-        if groups > 1:
-            send(0, 0, 0, full, across, y_slot)
-        to_sibling(0, 0, 0, full)
-        serve(per[0])
-        for s in range(1, highs):
-            arrived(0, s, 0, full, x_slot + s - 1)
+
+        def start():
+            if highs > 1:
+                send(0, 0, 0, full, x_next, x_slot)
             if groups > 1:
-                send(0, s, 0, half, across, top_slot + s - 1)
-            if s < highs - 1:
-                send(0, s, 0, full, x_next, x_slot + s)
-            to_sibling(0, s, 0, full)
-        if groups > 1:
-            arrived(1, 0, 0, full, y_slot)
-            if highs > 1:
-                send(1, 0, half, half, x_next, low_slot)
-            to_sibling(1, 0, 0, full)
-            serve(per[1])
+                send(0, 0, 0, full, across, y_slot)
+            to_sibling(0, 0, 0, full)
+
+        def turn():
             for s in range(1, highs):
-                arrived(1, s, half, half, low_slot + s - 1)
+                arrived(0, s, 0, full, x_slot + s - 1)
+                if groups > 1:
+                    send(0, s, 0, half, across, top_slot + s - 1)
                 if s < highs - 1:
-                    send(1, s, half, half, x_next, low_slot + s)
-                to_sibling(1, s, half, half)
-                arrived(1, s, 0, half, top_slot + s - 1)
-                to_sibling(1, s, 0, half)
-        for g, s, offset, size, slot in expected:
-            arrived(g, s, offset, size, slot, 1 - my_low)
-
+                    send(0, s, 0, full, x_next, x_slot + s)
+                to_sibling(0, s, 0, full)
+            if groups > 1:
+                arrived(1, 0, 0, full, y_slot)
+                if highs > 1:
+                    send(1, 0, half, half, x_next, low_slot)
+                to_sibling(1, 0, 0, full)
+
+        def finish():
+            if groups > 1:
+                for s in range(1, highs):
+                    arrived(1, s, half, half, low_slot + s - 1)
+                    if s < highs - 1:
+                        send(1, s, half, half, x_next, low_slot + s)
+                    to_sibling(1, s, half, half)
+                    arrived(1, s, 0, half, top_slot + s - 1)
+                    to_sibling(1, s, 0, half)
+            for g, s, offset, size, slot in expected:
+                arrived(g, s, offset, size, slot, 1 - my_low)
+
+        return start, turn, finish
+
+    def part_gather(index, part):
+        def place(g, t, offset, size):
+            return column_place(g, t, part * rows + offset, size)
+
+        return gather(index, index * groups + part, place, rows)
+
+    parts = range(groups)
     for m in range(ahead):
         w_own(m)
-    gather(0, token_place, rows, (2, 1))
-
+    start, turn, finish = gather(0, 0, token_place, rows)
+    start()
+    serve(2)
+    turn()
+    serve(1)
+    finish()
+    coming = [None] * groups
+
+    chunks = rows // chunk
     for layer in range(layers):
         now, mixed_at = 2 * layer, 2 * layer + 1
         first = layer * KINDS
@@ -210,8 +232,7 @@
             serve_until(first + j)
 
         def project(g, c):
-            start = g * rows + c * chunk
-            picked = pl.ds(pl.multiple_of(start, chunk), chunk)
+            picked = pl.ds(pl.multiple_of(g * rows + c * chunk, chunk), chunk)
             x = acts[now, picked, :].astype(jnp.float32)
             factor = lax.rsqrt(jnp.mean(x * x, axis=1, keepdims=True) + EPS)
             normed = (x * factor * gain[layer : layer + 1, :].astype(jnp.float32)).astype(jnp.bfloat16)
@@ -221,34 +242,21 @@
             carried[g, pl.ds(pl.multiple_of(8 + c * chunk, 8), chunk), :] = (
                 inner.astype(jnp.float32) * values.astype(jnp.float32))
 
-        chunks = rows // chunk
-
-        @pl.loop(0, groups * chunks)
-        def _(i):
-            project(lax.rem(i, groups), chunks - 1 - i // groups)
-
-        for g in range(groups):
-            edge_out[layer, g] = carried[g, 8 + rows - reach : 8 + rows, :]
-        edge = pltpu.make_async_remote_copy(
-            src_ref=edge_out.at[layer], dst_ref=edge_in.at[layer], send_sem=e_send.at[layer],
-            recv_sem=e_recv.at[layer], device_id=right, device_id_type=MESH)
-
-        @pl.when(me < n - 1)
-        def _():
-            edge.start()
-
-        @pl.when(me == 0)
-        def _():
-            for g in range(groups):
+        def edge(g):
+            return pltpu.make_async_remote_copy(
+                src_ref=edge_out.at[layer, g], dst_ref=edge_in.at[layer, g], send_sem=e_send.at[layer, g],
+                recv_sem=e_recv.at[layer, g], device_id=right, device_id_type=MESH)
+
+        def convolve(g):
+            @pl.when(me == 0)
+            def _():
                 carried[g, 8 - reach : 8, :] = jnp.zeros((reach, width), jnp.float32)
 
-        @pl.when(me > 0)
-        def _():
-            edge.wait_recv()
-            for g in range(groups):
+            @pl.when(me > 0)
+            def _():
+                edge(g).wait_recv()
                 carried[g, 8 - reach : 8, :] = edge_in[layer, g]
 
-        for g in range(groups):
             conv = jnp.zeros((rows, width), jnp.float32)
             for tap in range(reach + 1):
                 row = taps[layer, tap : tap + 1, own_columns].astype(jnp.float32)
@@ -256,26 +264,57 @@
             acts[mixed_at, g * rows : (g + 1) * rows, own] = (
                 gates[g * rows : (g + 1) * rows, :].astype(jnp.float32) * conv).astype(jnp.bfloat16)
 
-        gather(mixed_at, column_place, all_rows, (2, 1))
-        serve_until(first + 3)
+        going = [part_gather(mixed_at, g) for g in parts]
+        for g in parts:
+            if coming[g] is not None:
+                coming[g][2]()
+
+            @pl.loop(0, chunks)
+            def _(i):
+                project(g, i)
+
+            edge_out[layer, g] = carried[g, 8 + rows - reach : 8 + rows, :]
+
+            @pl.when(me < n - 1)
+            def _():
+                edge(g).start()
+
+            if g > 0:
+                convolve(g - 1)
+                going[g - 1][0]()
+        convolve(groups - 1)
+        going[groups - 1][0]()
 
         if layer == 0:
             own_now = pl.ds(pl.multiple_of(my_tp * block_width + my_grp * width, width), width)
         else:
             own_now = own
-
-        @pl.loop(0, all_rows // chunk)
-        def _(c):
-            picked = pl.ds(pl.multiple_of(c * chunk, chunk), chunk)
-            product = jnp.dot(acts[mixed_at, picked, :], wide[first + 3], preferred_element_type=jnp.float32)
-            stream = (acts[now, picked, own_now].astype(jnp.float32) + product).astype(jnp.bfloat16)
+        coming = [part_gather(now + 2, g) if layer < layers - 1 else None for g in parts]
+        for g in parts:
+            serve(2)
+            going[g][1]()
+        serve(1)
+        for g in parts:
+            going[g][2]()
+            serve_until(first + 3)
+
+            @pl.loop(0, chunks)
+            def _(c):
+                picked = pl.ds(pl.multiple_of(g * rows + c * chunk, chunk), chunk)
+                product = jnp.dot(acts[mixed_at, picked, :], wide[first + 3], preferred_element_type=jnp.float32)
+                stream = (acts[now, picked, own_now].astype(jnp.float32) + product).astype(jnp.bfloat16)
+                if layer < layers - 1:
+                    acts[now + 2, picked, own] = stream
+                else:
+                    last[picked, :] = stream
+
             if layer < layers - 1:
-                acts[now + 2, picked, own] = stream
-            else:
-                last[picked, :] = stream
-
+                coming[g][0]()
         if layer < layers - 1:
-            gather(now + 2, column_place, all_rows, (3, 3))
+            for g in parts:
+                serve(2)
+                coming[g][1]()
+            serve(1)
 
     mine = pl.ds(pl.multiple_of(my_grp * rows, rows), rows)
     if groups > 1:
@@ -294,11 +333,12 @@
     for c in sends:
         c.wait_send()
     for layer in range(layers):
-        @pl.when(me < n - 1)
-        def _(layer=layer):
-            pltpu.make_async_remote_copy(
-                src_ref=edge_out.at[layer], dst_ref=edge_in.at[layer], send_sem=e_send.at[layer],
-                recv_sem=e_recv.at[layer], device_id=right, device_id_type=MESH).wait_send()
+        for g in parts:
+            @pl.when(me < n - 1)
+            def _(layer=layer, g=g):
+                pltpu.make_async_remote_copy(
+                    src_ref=edge_out.at[layer, g], dst_ref=edge_in.at[layer, g], send_sem=e_send.at[layer, g],
+                    recv_sem=e_recv.at[layer, g], device_id=right, device_id_type=MESH).wait_send()
     for m in range(total):
         for k in range(n):
             @pl.when((me - k >= 0) & (me < n - 1))
@@ -342,10 +382,10 @@
             dma((total + 1,)),
             dma((total, 2, n)),
             dma((total, n)),
-            dma((2 * layers, slots)),
-            dma((2 * layers, slots)),
-            dma((layers,)),
-            dma((layers,)),
+            dma((2 * layers * groups, slots)),
+            dma((2 * layers * groups, slots)),
+            dma((layers, groups)),
+            dma((layers, groups)),
             dma,
             dma,
         ],

time: 176 us -> 170 us (0.966)
  Pallas kernels: 173 us -> 166 us
    pallas_call x1, Pallas kernels: 173 us -> 166 us  [shards(): pl.pallas_call(functools.partial(kernel, (groups, n, tps, lows)), out_sha...]
where the time goes in v2:
time: 170 us; the launch traced here: 169 us
  Pallas kernels  166 us (98%)
  local copies, waits for them, and re-layouts  3.16 us (2%)
    pallas_call x1, Pallas kernels, shards(): pl.pallas_call(functools.partial(kernel, (groups, n, tps, lows)), out_sha...  166 us

profile of v2, /device:TPU:0, one launch (start us, length us, event | category | flops | bytes accessed | tf_op | source)
XLA Modules:
  0.0 169.2 jit_solution(5646389836206589613)
XLA Ops:
  0.0 1.3 copy.8.taps
  1.3 166.1 %mixers.1 = bf16[512,512]{1,0:T(8,128)(2,1)} custom-call(bf16[512,512]{1,0:T(8,128)(2,1)} %tokens.1, bf16[2,2048]{1,0:T(2,128)(2,1)} %gain.1, bf16[2,512,512]{2,1,0:T(8,128)(2,1)} %gate_w.1, bf16[2,512,512]{2,1,0:T(8,128)(2,1)} %mix_w.1, bf16[2,512,512]{2,1,0:T(8,128)(2,1)} %value_w.1, bf16[2,512,512]{2,1,0:T(8,128)(2,1)} %out_w.1, bf16[2,3,512]{2,1,0:T(4,128)(2,1)} %copy.8.taps), custom_call_target="tpu_custom_call" | custom-call | tf_op jit(solution)/shard_map/mixers/pallas_call | solution.py:368
  167.4 1.9 %copy.10 = bf16[512,512]{1,0:T(8,128)(2,1)} copy(bf16[512,512]{1,0:T(8,128)(2,1)} %mixers.1) | data formatting | bytes 1048576

commit v3 on v2

--- a/solution.py
+++ b/solution.py
@@ -76,7 +76,7 @@
             weights[m % KINDS].at[m // KINDS, :, own_columns], wide.at[m, w_rows(me), :], local_sem.at[m + 1]))
     for copy in locals_:
         copy.start()
-    for copy in locals_:
+    for copy in locals_[:4]:
         copy.wait()
 
     pl.semaphore_wait(barrier, len(fixed) + jnp.minimum(me, 1) + jnp.minimum(n - 1 - me, 1))
@@ -218,6 +218,8 @@
         w_own(m)
     start, turn, finish = gather(0, 0, token_place, rows)
     start()
+    for copy in locals_[4:]:
+        copy.wait()
     serve(2)
     turn()
     serve(1)

time: 170 us -> 169 us (level)
  no operation moved by 1% of the time
where the time goes in v3:
time: 169 us
  Pallas kernels  166 us (98%)
  local copies, waits for them, and re-layouts  3.16 us (2%)
    pallas_call x1, Pallas kernels, shards(): pl.pallas_call(functools.partial(kernel, (groups, n, tps, lows)), out_sha...  166 us

profile of v3, /device:TPU:0, one launch (start us, length us, event | category | flops | bytes accessed | tf_op | source)
XLA Modules:
  0.0 169.1 jit_solution(1540907082487190280)
XLA Ops:
  0.0 1.3 copy.8.taps
  1.3 166.0 %mixers.1 = bf16[512,512]{1,0:T(8,128)(2,1)} custom-call(bf16[512,512]{1,0:T(8,128)(2,1)} %tokens.1, bf16[2,2048]{1,0:T(2,128)(2,1)} %gain.1, bf16[2,512,512]{2,1,0:T(8,128)(2,1)} %gate_w.1, bf16[2,512,512]{2,1,0:T(8,128)(2,1)} %mix_w.1, bf16[2,512,512]{2,1,0:T(8,128)(2,1)} %value_w.1, bf16[2,512,512]{2,1,0:T(8,128)(2,1)} %out_w.1, bf16[2,3,512]{2,1,0:T(4,128)(2,1)} %copy.8.taps), custom_call_target="tpu_custom_call" | custom-call | tf_op jit(solution)/shard_map/mixers/pallas_call | solution.py:370
  167.3 1.9 %copy.10 = bf16[512,512]{1,0:T(8,128)(2,1)} copy(bf16[512,512]{1,0:T(8,128)(2,1)} %mixers.1) | data formatting | bytes 1048576
